TPU v7x, 32 devices: a whole 2x2x4 slice. The times are simulated.
32 devices in a mesh: ep: 8 (over z, x), tp: 4 (over y, core).
Axes of the slice: x: 2, y: 2, z: 4, core: 2. Of those that a mesh axis runs over, the one named last changes fastest.
Arguments:
- mix_in: bfloat16 [1024, 2048], P('ep'), may hold values from -6 to 6
- mix_gain: float32 [2048], replicated, may hold values from 0.1 to 1.9
- query_weight: bfloat16 [2048, 3072], P(None, 'tp'), may hold values from -0.125 to 0.125
- latent_weight: bfloat16 [2048, 512], replicated, may hold values from -0.125 to 0.125
- rotary_weight: bfloat16 [2048, 64], replicated, may hold values from -0.125 to 0.125
- latent_gain: float32 [512], replicated, may hold values from 0.1 to 1.9
- key_weight: bfloat16 [512, 2048], P(None, 'tp'), may hold values from -0.25 to 0.25
- value_weight: bfloat16 [512, 2048], P(None, 'tp'), may hold values from -0.25 to 0.25
- output_weight: bfloat16 [2048, 2048], P('tp'), may hold values from -0.125 to 0.125
- out_gain: float32 [2048], replicated, may hold values from 0.1 to 1.9
- ffn_in: bfloat16 [1024, 2048], P('ep'), may hold values from -6 to 6
- ffn_gain: float32 [2048], replicated, may hold values from 0.1 to 1.9
- gate_weight: bfloat16 [8, 2048, 1024], P('ep', None, 'tp'), may hold values from -0.375 to 0.375
- up_weight: bfloat16 [8, 2048, 1024], P('ep', None, 'tp'), may hold values from -0.375 to 0.375
- down_weight: bfloat16 [8, 1024, 2048], P('ep', 'tp'), may hold values from -0.046875 to 0.046875
- routes: int32 [1024, 4], P('ep'), may hold values from 0 to 7, all different within a row; in each aligned block of 32 rows (0 to 31, 32 to 63, ...) at most 32 rows name the same one
- route_scores: float32 [1024, 4], P('ep'), may hold values from -6 to 6
Outputs:
- mixed: bfloat16 [1024, 2048], P(('ep', 'tp'))
- moe_out: bfloat16 [1024, 2048], P(('ep', 'tp'))
Inputs may be any that keep to these rules, and one draw needn't show every extreme that they name: `routes`: each row names 4 different experts; in each aligned block of 32 rows no expert is named by more than 32 rows, a bound that some blocks reach.
All inputs are finite; a program needn't handle non-finite values.
Results may differ from a plain program's by a relative error of at most 0.014.
Values may be sent and summed in bfloat16 or wider, within the bound.
A program may use at most 192 MiB of HBM per device.

v0:
```python
import jax
import jax.numpy as jnp
from jax import lax
from jax.sharding import PartitionSpec as P

NOPE = 128
ROPE = 64
VD = 128


norm_eps = 1e-06
clamp_limit = 7.0
gate_slope = 1.702
rope_base = 10000.0


def rms_rows(rows_in, scales):
    mean_square = jnp.mean(rows_in * rows_in, axis=-1, keepdims=True)
    return rows_in * lax.rsqrt(mean_square + norm_eps) * scales


def rms_columns(columns, scales):
    mean_square = jnp.mean(columns * columns, axis=0, keepdims=True)
    return columns * lax.rsqrt(mean_square + norm_eps) * scales[:, None]


def turn_table(positions):
    inverse = rope_base ** (-jnp.arange(0, ROPE, 2).astype(jnp.float32) / ROPE)
    angle_rows = inverse[:, None] * positions.astype(jnp.float32)[None, :]
    return (jnp.cos(angle_rows), jnp.sin(angle_rows))


def clamped_unit(gate_part, linear):
    gate_part = jnp.minimum(gate_part, clamp_limit)
    linear = jnp.clip(linear, -clamp_limit, clamp_limit)
    return gate_part * jax.nn.sigmoid(gate_slope * gate_part) * (linear + 1.0)


def keep_state(running):
    return running


def local(
    mix_in,
    mix_gain,
    query_weight,
    latent_weight,
    rotary_weight,
    latent_gain,
    key_weight,
    value_weight,
    output_weight,
    out_gain,
    ffn_in,
    ffn_gain,
    gate_weight,
    up_weight,
    down_weight,
    routes,
    route_scores,
):
    row_count = mix_in.shape[0]
    first_row = lax.axis_index("ep") * row_count
    last_row = first_row + row_count - 1
    positions = first_row + jnp.arange(row_count, dtype=jnp.int32)
    normed = rms_rows(mix_in.astype(jnp.float32), mix_gain).astype(jnp.bfloat16)
    head_count = query_weight.shape[1] // (NOPE + ROPE)
    half_rope = ROPE // 2
    cosine, sine_rows = turn_table(positions)
    queries = jnp.dot(normed, query_weight, preferred_element_type=jnp.float32).reshape(
        row_count, head_count, NOPE + ROPE
    )
    query_plain = queries[..., :NOPE].astype(jnp.bfloat16)
    query_cos = cosine.T[:, None, :]
    query_sin = sine_rows.T[:, None, :]
    query_upper = queries[..., NOPE : NOPE + half_rope]
    query_lower = queries[..., NOPE + half_rope :]
    query_turn = jnp.concatenate(
        [
            query_upper * query_cos - query_lower * query_sin,
            query_lower * query_cos + query_upper * query_sin,
        ],
        axis=-1,
    ).astype(jnp.bfloat16)
    across = (((0,), (1,)), ((), ()))
    latent = rms_columns(
        lax.dot_general(latent_weight, normed, across, preferred_element_type=jnp.float32),
        latent_gain,
    ).astype(jnp.bfloat16)
    rot_raw = lax.dot_general(rotary_weight, normed, across, preferred_element_type=jnp.float32)
    rotary_key = jnp.concatenate(
        [
            rot_raw[:half_rope] * cosine - rot_raw[half_rope:] * sine_rows,
            rot_raw[half_rope:] * cosine + rot_raw[:half_rope] * sine_rows,
        ],
        axis=0,
    ).astype(jnp.bfloat16)
    score_scale = (NOPE + ROPE) ** (-0.5)
    contract_first = (((0,), (0,)), ((), ()))

    def expand(latent_block):
        key_block = lax.dot_general(
            key_weight, latent_block, contract_first, preferred_element_type=jnp.float32
        ).astype(jnp.bfloat16)
        value_block = lax.dot_general(
            value_weight, latent_block, contract_first, preferred_element_type=jnp.float32
        ).astype(jnp.bfloat16)
        return (key_block, value_block)

    def attend(key_block, value_block, turn_block):
        key_count = key_block.shape[1]
        key_block = key_block.reshape(head_count, NOPE, key_count)
        value_block = value_block.reshape(head_count, VD, key_count)
        scores = jnp.einsum(
            "ihd,hdj->hij", query_plain, key_block, preferred_element_type=jnp.float32
        )
        scores = scores + jnp.einsum(
            "ihd,dj->hij", query_turn, turn_block, preferred_element_type=jnp.float32
        )
        key_places = jnp.arange(key_count, dtype=jnp.int32)
        allowed = key_places[None, :] <= positions[:, None]
        weights = jnp.where(allowed[None], jnp.exp(scores * score_scale), 0.0)
        weighted = jnp.einsum(
            "hij,hdj->hid",
            weights.astype(jnp.bfloat16),
            value_block,
            preferred_element_type=jnp.float32,
        )
        return (jnp.sum(weights, axis=-1), weighted)

    initial = (
        jnp.zeros((head_count, row_count), jnp.float32),
        jnp.zeros((head_count, row_count, VD), jnp.float32),
    )
    shard_piece = (
        lax.all_gather(latent, "ep", axis=1, tiled=True),
        lax.all_gather(rotary_key, "ep", axis=1, tiled=True),
    )

    def compute_piece(running):
        key_block, value_block = expand(shard_piece[0])
        return attend(key_block, value_block, shard_piece[1])

    totals, weighted = lax.cond(jnp.int32(0) > last_row, keep_state, compute_piece, initial)
    attended = (weighted / totals[..., None]).astype(jnp.bfloat16)
    mixing = output_weight.reshape(head_count, VD, output_weight.shape[1])
    partial_value = jnp.einsum("hid,hde->ie", attended, mixing, preferred_element_type=jnp.float32)
    projected = lax.psum_scatter(
        lax.optimization_barrier(partial_value.astype(jnp.bfloat16))
        .astype(jnp.float32)
        .astype(jnp.bfloat16),
        "tp",
        scatter_dimension=0,
        tiled=True,
    ).astype(jnp.float32)
    mixed = rms_rows(projected, out_gain).astype(jnp.bfloat16)
    tokens = ffn_in.shape[0]
    part_count = lax.axis_size("tp")
    quarter_rows = tokens // part_count
    experts = lax.axis_size("ep")
    choose = routes.shape[1]
    capacity = max(2, 2 * quarter_rows * choose // experts)
    slot_count = capacity * part_count
    tp_index = lax.axis_index("tp")
    normed_b = rms_rows(ffn_in.astype(jnp.float32), ffn_gain).astype(jnp.bfloat16)
    padded = jnp.concatenate([normed_b, jnp.zeros((1, normed_b.shape[1]), jnp.bfloat16)], axis=0)
    gate_share = jax.nn.softmax(route_scores, axis=-1)
    grouped = routes.reshape(part_count, quarter_rows * choose)
    onehot = (grouped[:, :, None] == jnp.arange(experts, dtype=jnp.int32)[None, None, :]).astype(
        jnp.int32
    )
    slot_rank = jnp.sum((jnp.cumsum(onehot, axis=1) - 1) * onehot, axis=2)
    slot_index = jnp.arange(part_count, dtype=jnp.int32)[:, None] * capacity + slot_rank
    place_index = (slot_index * experts + grouped).reshape(-1)
    owners = jnp.arange(tokens * choose, dtype=jnp.int32) // choose
    slot_token = jnp.full((slot_count * experts,), tokens, jnp.int32).at[place_index].set(owners)
    unit_count = gate_weight.shape[2]
    chosen = lax.dynamic_slice_in_dim(
        slot_token, tp_index * capacity * experts, capacity * experts, 0
    )
    outgoing = padded[chosen].reshape(capacity, experts, -1)
    arrived = lax.all_to_all(outgoing, "ep", split_axis=1, concat_axis=1, tiled=True)
    row_block = lax.all_gather(arrived, "tp", axis=0, tiled=True)
    block_slots = row_block.shape[0]
    flat_rows = row_block.reshape(-1, row_block.shape[2])
    gate_part = jnp.dot(flat_rows, gate_weight[0], preferred_element_type=jnp.float32)
    up_part = jnp.dot(flat_rows, up_weight[0], preferred_element_type=jnp.float32)
    hidden = (
        clamped_unit(gate_part, up_part).astype(jnp.bfloat16).reshape(block_slots, -1, unit_count)
    )
    sources = hidden.shape[1]
    hidden_flat = hidden.reshape(slot_count * sources, unit_count)
    partial_value = jnp.dot(hidden_flat, down_weight[0], preferred_element_type=jnp.float32)
    result = lax.psum_scatter(
        lax.optimization_barrier(partial_value.astype(jnp.bfloat16))
        .astype(jnp.float32)
        .astype(jnp.bfloat16),
        "tp",
        scatter_dimension=0,
        tiled=True,
    )
    result = result.reshape(capacity, sources, -1)
    returned = lax.all_to_all(result, "ep", split_axis=1, concat_axis=1, tiled=True)
    back_rows = returned.reshape(capacity * experts, -1)
    own_rank = lax.dynamic_index_in_dim(slot_rank, tp_index, 0, keepdims=False)
    own_expert = lax.dynamic_index_in_dim(grouped, tp_index, 0, keepdims=False)
    picked = (
        back_rows[own_rank * experts + own_expert]
        .astype(jnp.float32)
        .reshape(quarter_rows, choose, -1)
    )
    own_gates = lax.dynamic_slice_in_dim(gate_share, tp_index * quarter_rows, quarter_rows, 0)
    moe_out = jnp.sum(picked * own_gates[:, :, None], axis=1).astype(jnp.bfloat16)
    return (mixed, moe_out)


def solution(mesh):
    placed = (
        P("ep", None),
        P(),
        P(None, "tp"),
        P(),
        P(),
        P(),
        P(None, "tp"),
        P(None, "tp"),
        P("tp", None),
        P(),
        P("ep", None),
        P(),
        P("ep", None, "tp"),
        P("ep", None, "tp"),
        P("ep", "tp", None),
        P("ep", None),
        P("ep", None),
    )
    return jax.shard_map(
        local,
        mesh=mesh,
        in_specs=placed,
        out_specs=(P(("ep", "tp"), None), P(("ep", "tp"), None)),
        check_vma=False,
    )
```

profile of v0, /device:TPU:0, one launch (start us, length us, event | category | flops | bytes accessed | tf_op | source)
XLA Modules:
  0.0 232.8 jit_solution(3613812320336969351)
XLA Ops:
  7.2 0.0 copy-start
  7.2 0.0 all-gather.5.cloned.1.call-start
  7.2 0.9 copy.41
  8.2 0.1 eq.15
  8.3 0.1 reshape.243
  8.4 0.8 fusion.52
  9.2 1.2 reduce_window_sum.11
  10.5 0.2 select_reduce_fusion
  10.7 0.1 add_multiply_fusion
  10.8 2.5 %scatter_custom_fusion = s32[1024]{0:T(1024)S(1)} fusion(s32[512]{0:T(512)S(1)} %bitcast.86, s32[512]{0:T(512)S(1)} %add_select_fusion, s32[]{:T(128)} %constant.36.clone.1), kind=kCustom, calls=%fused_computation.95 | custom fusion | bytes 4100 | tf_op jit(solution)/shard_map/scatter | solution.py:176
  13.2 0.1 compare_select_fusion.1
  13.3 1.2 fusion.32
  14.6 1.2 fusion.34
  15.8 0.9 concatenate.13
  16.7 4.5 %gather_fusion = bf16[256,2048]{1,0:T(8,128)(2,1)} fusion(bf16[129,2048]{1,0:T(8,128)(2,1)} %concatenate.13, s32[1024]{0:T(1024)S(1)} %pad_clamp_fusion.1), kind=kCustom, calls=%fused_computation | custom fusion | bytes 2098176 | tf_op jit(solution)/shard_map/gather | solution.py:181
  21.2 1.8 copy.43
  23.0 32.8 %all_to_all.10 = bf16[32,8,2048]{2,0,1:T(8,128)(2,1)S(1)} all-to-all(bf16[32,8,2048]{2,0,1:T(8,128)(2,1)S(1)} %copy.43), channel_id=1, replica_groups=mesh['ep'=8,'tp'=4] {'ep'}, dimensions={1} | all-to-all | bytes 2097152 | tf_op jit(solution)/shard_map/all_to_all | solution.py:182
  55.8 1.6 copy.44
  57.4 0.0 all-gather.5.cloned.1.call-update
  57.4 0.0 all-gather.3.cloned.1.call-start
  57.5 1.2 fusion.29
  58.7 0.0 copy-start.7
  58.7 2.3 %multiply_reduce_fusion.1 = (f32[128]{0:T(128)S(1)}, f32[128,512]{1,0:T(8,128)S(1)}) fusion(bf16[2048,512]{1,0:T(8,128)(2,1)} %param.22, bf16[128,2048]{1,0:T(8,128)(2,1)} %param.19, f32[2048]{0:T(1024)S(1)} %copy-done.4, f32[128]{0:T(128)S(1)} %add_rsqrt_fusion.3), kind=kOutput, calls=%fused_computation.63 | convolution fusion | flops 269614976 | bytes 2892800 | tf_op jit(solution)/shard_map/dot_general | solution.py:87
  61.1 0.7 fusion.53
  61.8 0.0 all-gather.3.cloned.1.call-update
  61.8 0.0 reduce-scatter.5.cloned.1.call-start
  61.9 29.2 %all-gather.5.cloned.1.call-done = bf16[128,8,2048]{2,1,0:T(8,128)(2,1)} async-done(((bf16[32,8,2048]{2,1,0:T(8,128)(2,1)}), bf16[128,8,2048]{2,1,0:T(8,128)(2,1)}) %all-gather.5.cloned.1.call-update) | async-done | bytes 4194320 | tf_op jit(solution)/shard_map/all_gather | solution.py:183
  91.1 4.7 %fusion.12 = f32[1024,256]{1,0:T(8,128)} fusion(bf16[128,8,2048]{2,1,0:T(8,128)(2,1)} %all-gather.5.cloned.1.call-done, bf16[1,2048,256]{2,1,0:T(8,128)(2,1)} %param.31), kind=kOutput, calls=%fused_computation.22 | convolution fusion | flops 1074003968 | bytes 6291456 | tf_op jit(solution)/shard_map/dot_general | solution.py:186
  95.8 9.4 %convolution_convert_fusion.2 = bf16[1024,2048]{1,0:T(8,128)(2,1)} fusion(bf16[128,8,2048]{2,1,0:T(8,128)(2,1)} %all-gather.5.cloned.1.call-done, bf16[1,256,2048]{2,1,0:T(8,128)(2,1)} %param.33, bf16[1,2048,256]{2,1,0:T(8,128)(2,1)} %param.32, f32[1024,256]{1,0:T(8,128)} %fusion.12), kind=kOutput, calls=%fused_computation.19 | convolution fusion | flops 2151940096 | bytes 11534336 | tf_op jit(solution)/shard_map/dot_general | solution.py:193
  105.2 0.0 reduce-scatter.5.cloned.1.call-update
  105.2 0.0 reduce-scatter.3.cloned.1.call-start
  105.3 0.8 copy-done.11
  106.1 1.4 convolution_bitcast_fusion.1
  107.6 0.1 fusion.60
  107.7 27.7 %all_gather.10 = bf16[64,1024]{1,0:T(8,128)(2,1)} all-gather(bf16[64,128]{1,0:T(8,128)(2,1)S(1)} %pad_maximum_fusion.1), channel_id=1, replica_groups=mesh['ep'=8,'tp'=4] {'ep'}, dimensions={1}, use_global_device_ids=true | all-gather | bytes 147456 | tf_op jit(solution)/shard_map/all_gather | solution.py:137
  135.4 0.5 iota_add_fusion
  136.0 0.1 multiply_cosine_fusion
  136.1 2.4 %fusion.79 = f32[128,768]{0,1:T(8,128)S(1)} fusion(bf16[2048,768]{1,0:T(8,128)(2,1)S(1)} %copy-done, bf16[128,2048]{1,0:T(8,128)(2,1)} %param.19, f32[2048]{0:T(1024)S(1)} %copy-done.4, f32[128]{0:T(128)} %copy-done.7), kind=kOutput, calls=%fused_computation.118 | convolution fusion | flops 403701760 | bytes 4071936 | tf_op jit(solution)/shard_map/dot_general | solution.py:70
  138.6 0.6 pad_maximum_fusion
  139.2 8.9 %conditional.1 = (f32[4,128]{1,0:T(4,128)S(1)}, f32[4,128,128]{2,1,0:T(8,128)S(1)}) conditional(s32[]{:T(128)} %convert_element_type.84, (s32[128]{0:T(128)}, bf16[512,512]{1,0:T(8,128)(2,1)}, bf16[512,1024]{0,1:T(8,128)(2,1)}, f32[128,4,192]{0,2,1:T(8,128)S(1)}, bf16[64,1024]{1,0:T(8,128)(2,1)}, /*index=5*/bf16[128,4,64]{0,2,1:T(8,128)(2,1)}, ...), branch_computations={%region_2.4_spmd, %region_4.5_spmd} | conditional | flops 1413086720 | bytes 22155932 | solution.py:144
  139.2 3.2 %convolution_convert_fusion.1 = bf16[512,1024]{1,0:T(8,128)(2,1)} fusion(bf16[512,512]{1,0:T(8,128)(2,1)} %get-tuple-element.30, bf16[512,1024]{0,1:T(8,128)(2,1)} %get-tuple-element.49), kind=kOutput, calls=%fused_computation.8 | convolution fusion | flops 537395200 | bytes 2621440 | tf_op jit(solution)/shard_map/cond/branch_0_fun/dot_general | solution.py:102
  142.4 0.8 copy.40
  143.2 2.1 fusion.5
  145.4 0.1 iota_compare_fusion
  145.5 0.8 fusion.83
  146.3 0.4 copy-done.9
  146.6 0.2 copy-done.10
  146.8 0.8 convolution_convert_fusion
  147.6 0.5 fusion.3
  148.1 2.9 %fusion.11 = bf16[128,2048]{1,0:T(8,128)(2,1)} fusion(bf16[4,128,2048]{2,1,0:T(8,128)(2,1)} %bitcast.81, f32[4,128,128]{2,1,0:T(8,128)S(1)} %get-tuple-element.25, f32[4,128]{1,0:T(4,128)S(1)} %get-tuple-element.26), kind=kOutput, calls=%fused_computation.21 | convolution fusion | flops 268828672 | bytes 2885632 | tf_op jit(solution)/shard_map/hid,hde->ie/dot_general | solution.py:147
  151.0 0.0 reduce-scatter.3.cloned.1.call-update
  151.0 29.7 %reduce-scatter.5.cloned.1.call-done = bf16[256,2048]{1,0:T(8,128)(2,1)} async-done(((bf16[1024,2048]{1,0:T(8,128)(2,1)}), bf16[256,2048]{1,0:T(8,128)(2,1)}) %reduce-scatter.5.cloned.1.call-update) | async-done | bytes 1048592 | tf_op jit(solution)/shard_map/reduce_scatter | solution.py:194
  180.7 2.9 %copy.45 = bf16[32,8,2048]{2,0,1:T(8,128)(2,1)} copy(bf16[32,8,2048]{2,1,0:T(8,128)(2,1)} %bitcast.83) | data formatting | bytes 2097152 | tf_op jit(solution)/shard_map/reshape | solution.py:202
  183.6 5.5 %all-to-all-start.1 = ((bf16[32,8,2048]{2,0,1:T(8,128)(2,1)}), bf16[32,8,2048]{2,0,1:T(8,128)(2,1)}, u32[]{:S(2)}, u32[]{:S(2)}) async-start(bf16[32,8,2048]{2,0,1:T(8,128)(2,1)} %copy.45), calls=%async_computation.3 | async-start | bytes 2097152 | tf_op jit(solution)/shard_map/all_to_all | solution.py:203
  189.2 0.1 constant_dynamic-slice_fusion.2
  189.2 0.1 copy.47
  189.4 15.4 %reduce-scatter.3.cloned.1.call-done = bf16[32,2048]{1,0:T(8,128)(2,1)} async-done(((bf16[128,2048]{1,0:T(8,128)(2,1)}), bf16[32,2048]{1,0:T(8,128)(2,1)}) %reduce-scatter.3.cloned.1.call-update) | async-done | bytes 131088 | tf_op jit(solution)/shard_map/reduce_scatter | solution.py:148
  204.8 1.0 fusion.49
  205.8 1.7 fusion.51
  207.5 7.4 %all-to-all-done.1 = bf16[32,8,2048]{2,0,1:T(8,128)(2,1)} async-done(((bf16[32,8,2048]{2,0,1:T(8,128)(2,1)}), bf16[32,8,2048]{2,0,1:T(8,128)(2,1)}, u32[]{:S(2)}, u32[]{:S(2)}) %all-to-all-start.1) | async-done | bytes 1048608 | tf_op jit(solution)/shard_map/all_to_all | solution.py:203
  214.9 2.8 %copy.53 = bf16[32,8,2048]{2,1,0:T(8,128)(2,1)} copy(bf16[32,8,2048]{2,0,1:T(8,128)(2,1)} %all-to-all-done.1) | data formatting | bytes 2097152 | tf_op jit(solution)/shard_map/all_to_all | solution.py:203
  217.7 3.6 %gather_fusion.1 = bf16[128,2048]{1,0:T(8,128)(2,1)} fusion(bf16[256,2048]{1,0:T(8,128)(2,1)} %bitcast.77, s32[1024]{0:T(1024)S(1)} %pad_clamp_fusion), kind=kCustom, calls=%fused_computation.1 | custom fusion | bytes 1049088 | tf_op jit(solution)/shard_map/gather | solution.py:208
  221.3 2.4 %reshape.248 = f32[32,4,2048]{2,1,0:T(4,128)} reshape(bf16[128,2048]{1,0:T(8,128)(2,1)} %gather_fusion.1) | data formatting | bytes 1572864 | tf_op jit(solution)/shard_map/convert_element_type | solution.py:209
  223.7 2.6 %multiply_reduce_fusion = bf16[32,2048]{1,0:T(8,128)(2,1)} fusion(f32[32,4,2048]{2,1,0:T(4,128)} %reshape.248, f32[32,4]{1,0:T(8,128)S(1)} %copy.47), kind=kLoop, calls=%fused_computation.42 | loop fusion | flops 458752 | bytes 1180160 | tf_op jit(solution)/shard_map/reduce_sum | solution.py:213
  (37 shorter events, 0.2 us)
Async XLA Ops:
  7.2 128.9 %copy-start = (bf16[2048,768]{1,0:T(8,128)(2,1)S(1)}, bf16[2048,768]{1,0:T(8,128)(2,1)}, u32[]{:S(2)}) copy-start(bf16[2048,768]{1,0:T(8,128)(2,1)} %param.21) | copy-start | bytes 9437188
  7.2 83.9 %all-gather.5.cloned.1.call-start = ((), (), s32[]{:S(2)}) async-start(), calls=%async_computation.6 | async-start | bytes 5242880 | tf_op jit(solution)/shard_map/all_gather | solution.py:183
  55.8 2.9 %copy-start.4 = (f32[2048]{0:T(1024)S(1)}, f32[2048]{0:T(1024)}, u32[]{:S(2)}) copy-start(f32[2048]{0:T(1024)} %param.20) | copy-start | bytes 24580
  57.4 3.7 %copy-start.6 = (f32[512]{0:T(512)S(1)}, f32[512]{0:T(512)}, u32[]{:S(2)}) copy-start(f32[512]{0:T(512)} %param.24) | copy-start | bytes 6148
  57.4 81.8 %all-gather.3.cloned.1.call-start = ((), (), s32[]{:S(2)}) async-start(), calls=%async_computation.4 | async-start | bytes 1179648 | tf_op jit(solution)/shard_map/all_gather | solution.py:136
  58.7 46.6 %copy-start.7 = (f32[128]{0:T(128)}, f32[128]{0:T(128)S(1)}, u32[]{:S(2)}) copy-start(f32[128]{0:T(128)S(1)} %add_rsqrt_fusion.3) | copy-start | bytes 1540
  61.8 118.9 %reduce-scatter.5.cloned.1.call-start = ((), (), s32[]{:S(2)}) async-start(), calls=%async_computation.7 | async-start | bytes 5242880 | tf_op jit(solution)/shard_map/reduce_scatter | solution.py:194
  105.2 0.9 copy-start.11
  105.2 99.6 %reduce-scatter.3.cloned.1.call-start = ((), (), s32[]{:S(2)}) async-start(), calls=%async_computation.5 | async-start | bytes 655360 | tf_op jit(solution)/shard_map/reduce_scatter | solution.py:148
  142.4 3.0 %copy-start.8 = (s32[128]{0:T(128)S(1)}, s32[128]{0:T(128)}, u32[]{:S(2)}) copy-start(s32[128]{0:T(128)} %get-tuple-element.14) | copy-start | bytes 1540 | tf_op jit(solution)/shard_map/cond
  143.2 2.3 copy-start.1
  143.2 2.3 copy-start.2
  145.3 1.3 copy-start.9
  145.4 1.5 copy-start.10
  180.7 8.4 %copy-start.3 = (f32[128,4]{0,1:T(4,128)S(1)}, f32[128,4]{0,1:T(4,128)}, u32[]{:S(2)}) copy-start(f32[128,4]{0,1:T(4,128)} %param.35) | copy-start | bytes 6148
  180.7 25.1 %copy-start.5 = (f32[2048]{0:T(1024)S(1)}, f32[2048]{0:T(1024)}, u32[]{:S(2)}) copy-start(f32[2048]{0:T(1024)} %param.28) | copy-start | bytes 24580
  183.6 31.3 %all-to-all-start.1 = ((bf16[32,8,2048]{2,0,1:T(8,128)(2,1)}), bf16[32,8,2048]{2,0,1:T(8,128)(2,1)}, u32[]{:S(2)}, u32[]{:S(2)}) async-start(bf16[32,8,2048]{2,0,1:T(8,128)(2,1)} %copy.45), calls=%async_computation.3 | async-start | bytes 2097152 | tf_op jit(solution)/shard_map/all_to_all | solution.py:203
Sparse Core Ops, SparseCore 0:
  57.5 33.4 all-gather.4
  93.8 40.4 all-gather.2
  136.8 43.9 reduce-scatter.4
  183.1 21.6 reduce-scatter.2
where the time goes:
time: 234 us; the launch traced here: 233 us
  waiting for transfers between devices  81.7 us (35%)
  blocking collectives  60.5 us (26%)
  matrix products  30.5 us (13%)
  local copies, waits for them, and re-layouts  26.4 us (11%)
  between operations  14 us (6%)
  other arithmetic  13.9 us (6%)
  starting transfers between devices  5.68 us (2%)
    reduce_scatter x2, waiting for transfers between devices, local(): lax.psum_scatter(lax.optimization_barrier(partial_value.astype(jnp.bfloat...  45.1 us
    all_to_all x1, blocking collectives, local(): lax.all_to_all(outgoing, 'ep', split_axis=1, concat_axis=1, tiled=True)  32.8 us
    all_gather x1, waiting for transfers between devices, local(): row_block = lax.all_gather(arrived, 'tp', axis=0, tiled=True)  29.2 us
    all_gather x1, blocking collectives, local(): lax.all_gather(rotary_key, 'ep', axis=1, tiled=True)  27.7 us
    dot_general x1, matrix products, local(): jnp.dot(hidden_flat, down_weight[0], preferred_element_type=jnp.float32)  9.41 us
    all_to_all x1, waiting for transfers between devices, local(): lax.all_to_all(result, 'ep', split_axis=1, concat_axis=1, tiled=True)  7.37 us
    all_to_all x1, starting transfers between devices, local(): lax.all_to_all(result, 'ep', split_axis=1, concat_axis=1, tiled=True)  5.52 us
    dot_general x1, matrix products, local(): jnp.dot(flat_rows, gate_weight[0], preferred_element_type=jnp.float32)  4.72 us
  transfers between devices with their start and end apart: 5, of which 4 were waited for; matrix products, arithmetic and copies ran while one was open for 18% of the time, Pallas kernels for 0%

commit v1 on v0

--- a/solution.py
+++ b/solution.py
@@ -1,6 +1,9 @@
 import jax
 import jax.numpy as jnp
+import functools
 from jax import lax
+from jax.experimental import pallas as pl
+from jax.experimental.pallas import tpu as pltpu
 from jax.sharding import PartitionSpec as P
 
 NOPE = 128
@@ -214,7 +217,329 @@
     return (mixed, moe_out)
 
 
+MESH = pl.DeviceIdType.MESH
+
+
+def flip(value, bits):
+    bit = 1
+    while bit <= bits:
+        if bits & bit:
+            value = value + bit - 2 * bit * ((value // bit) % 2)
+        bit *= 2
+    return value
+
+
+def here():
+    ep, tp = lax.axis_index("ep"), lax.axis_index("tp")
+    return ep // 2, ep % 2, tp // 2, tp % 2
+
+
+def place(z, x, y, core):
+    return {"ep": z * 2 + x, "tp": y * 2 + core}
+
+
+def greet(partners):
+    barrier = pltpu.get_barrier_semaphore()
+    for partner in partners:
+        pl.semaphore_signal(barrier, inc=1, device_id=partner, device_id_type=MESH)
+    pl.semaphore_wait(barrier, len(partners))
+
+
+def gather_kernel(depth, row_ref, side_ref, rows_out, side_out, send_sem, recv_sem):
+    z, x, y, core = here()
+    x_next, y_next, twin = place(z, 1 - x, y, core), place(z, x, 1 - y, core), place(z, x, y, 1 - core)
+    columns = [place(flip(z, d), x, y, core) for d in range(1, depth)]
+    greet(columns + [x_next, y_next, twin])
+    started = []
+
+    def copies(origin, target, own):
+        e, t = origin["ep"], origin["tp"]
+        number = len(started)
+        return [
+            pltpu.make_async_remote_copy(
+                src_ref=mine if own else out.at[e, t],
+                dst_ref=out.at[e, t],
+                send_sem=send_sem.at[a, number],
+                recv_sem=recv_sem.at[a, e, t],
+                device_id=target,
+                device_id_type=MESH,
+            )
+            for a, (mine, out) in enumerate(((side_ref, side_out), (row_ref, rows_out)))
+        ]
+
+    def send(origin, target, own=False):
+        pair = copies(origin, target, own)
+        for copy in pair:
+            copy.start()
+        started.append(pair)
+
+    def arrive(origin):
+        for copy in copies(origin, twin, False):
+            copy.wait_recv()
+
+    me = place(z, x, y, core)
+    for target in columns + [x_next, y_next, twin]:
+        send(me, target, True)
+    rows_out[me["ep"], me["tp"]] = row_ref[...]
+    side_out[me["ep"], me["tp"]] = side_ref[...]
+
+    def square(d):
+        at = flip(z, d)
+        from_x, from_y = place(at, 1 - x, y, core), place(at, x, 1 - y, core)
+        arrive(from_x)
+        if d % 2 == 0:
+            send(from_x, y_next)
+        send(from_x, twin)
+        arrive(from_y)
+        if d % 2 == 1:
+            send(from_y, x_next)
+        send(from_y, twin)
+
+    for d in range(1, depth):
+        origin = place(flip(z, d), x, y, core)
+        arrive(origin)
+        for target in (x_next, y_next, twin):
+            send(origin, target)
+        square(d - 1)
+    square(depth - 1)
+    for d in range(depth):
+        origin = place(flip(z, d), 1 - x, 1 - y, core)
+        arrive(origin)
+        send(origin, twin)
+    for d in range(depth):
+        for a in (x, 1 - x):
+            for b in (y, 1 - y):
+                arrive(place(flip(z, d), a, b, 1 - core))
+    for pair in started:
+        for copy in pair:
+            copy.wait_send()
+
+
+def gather_blocks(rows, side, experts, parts):
+    depth = experts // 2
+    sends = depth + 2 + 3 * (depth - 1) + 3 * depth + depth
+    whole = [jax.ShapeDtypeStruct((experts, parts) + a.shape, a.dtype) for a in (rows, side)]
+    vmem = pl.BlockSpec(memory_space=pltpu.VMEM)
+    return pl.pallas_call(
+        functools.partial(gather_kernel, depth),
+        out_shape=whole,
+        in_specs=[vmem] * 2,
+        out_specs=[vmem] * 2,
+        scratch_shapes=[
+            pltpu.SemaphoreType.DMA((2, sends)),
+            pltpu.SemaphoreType.DMA((2, experts, parts)),
+        ],
+        compiler_params=pltpu.CompilerParams(
+            collective_id=0, has_side_effects=True, vmem_limit_bytes=48 * 1024 * 1024
+        ),
+        name="gather_blocks",
+    )(rows, side)
+
+
+def reduce_kernel(
+    depth, part_ref, heads_ref, gain_ref, mixed_ref, moe_ref,
+    work, twin_in, hop_in, direct_in, relay_in, column_in,
+    heads_work, heads_twin, heads_in, send_sem, twin_sem, square_sem, column_sem, heads_sem,
+):
+    z, x, y, core = here()
+    x_next, y_next, twin = place(z, 1 - x, y, core), place(z, x, 1 - y, core), place(z, x, y, 1 - core)
+    columns = [place(flip(z, d), x, y, core) for d in range(1, depth)]
+    greet(columns + [x_next, y_next, twin])
+    started = []
+
+    def make(src, dst, sem, target):
+        return pltpu.make_async_remote_copy(
+            src_ref=src, dst_ref=dst, send_sem=send_sem.at[len(started)], recv_sem=sem,
+            device_id=target, device_id_type=MESH,
+        )
+
+    def send(src, dst, sem, target):
+        copy = make(src, dst, sem, target)
+        copy.start()
+        started.append(copy)
+
+    def arrive(dst, sem):
+        make(dst, dst, sem, twin).wait_recv()
+
+    def mine(d, a, b):
+        return part_ref[flip(z, d) * 2 + flip(x, a), flip(y, b) * 2 + core].astype(jnp.float32)
+
+    order = list(range(1, depth)) + [0]
+    for b in (1, 0):
+        send(heads_ref.at[flip(y, b) * 2 + 1 - core], heads_twin.at[b], heads_sem.at[b], twin)
+    turns = [(1, 1), (1, 0), (0, 1), (0, 0)]
+    for d in order:
+        for a, b in turns:
+            e, t = flip(z, d) * 2 + flip(x, a), flip(y, b) * 2 + 1 - core
+            send(part_ref.at[e, t], twin_in.at[d, a, b], twin_sem.at[d, a, b], twin)
+
+    arrive(heads_twin.at[1], heads_sem.at[1])
+    heads_work[...] = (
+        heads_ref[(1 - y) * 2 + core].astype(jnp.float32) + heads_twin[1].astype(jnp.float32)
+    ).astype(jnp.bfloat16)
+    send(heads_work, heads_in, heads_sem.at[2], y_next)
+
+    def paired(d, a, b):
+        arrive(twin_in.at[d, a, b], twin_sem.at[d, a, b])
+        return mine(d, a, b) + twin_in[d, a, b].astype(jnp.float32)
+
+    for d in order:
+        work[d, 1, 1] = paired(d, 1, 1).astype(jnp.bfloat16)
+        send(work.at[d, 1, 1], hop_in.at[d], square_sem.at[0, d], y_next if d % 2 else x_next)
+        a, b = (0, 1) if d % 2 else (1, 0)
+        work[d, a, b] = paired(d, a, b).astype(jnp.bfloat16)
+        send(work.at[d, a, b], direct_in.at[d], square_sem.at[1, d], y_next if d % 2 else x_next)
+    for d in order:
+        a, b = (1, 0) if d % 2 else (0, 1)
+        value = paired(d, a, b)
+        arrive(hop_in.at[d], square_sem.at[0, d])
+        work[d, a, b] = (value + hop_in[d].astype(jnp.float32)).astype(jnp.bfloat16)
+        send(work.at[d, a, b], relay_in.at[d], square_sem.at[2, d], x_next if d % 2 else y_next)
+    for d in order:
+        value = paired(d, 0, 0)
+        arrive(direct_in.at[d], square_sem.at[1, d])
+        value = value + direct_in[d].astype(jnp.float32)
+        arrive(relay_in.at[d], square_sem.at[2, d])
+        value = value + relay_in[d].astype(jnp.float32)
+        if d:
+            work[d, 0, 0] = value.astype(jnp.bfloat16)
+            send(work.at[d, 0, 0], column_in.at[d], column_sem.at[d], columns[d - 1])
+        else:
+            total = value
+    arrive(heads_twin.at[0], heads_sem.at[0])
+    arrive(heads_in, heads_sem.at[2])
+    projected = (
+        heads_ref[y * 2 + core].astype(jnp.float32)
+        + heads_twin[0].astype(jnp.float32)
+        + heads_in[...].astype(jnp.float32)
+    )
+    mixed_ref[...] = rms_rows(projected, gain_ref[...]).astype(jnp.bfloat16)
+    for d in range(1, depth):
+        arrive(column_in.at[d], column_sem.at[d])
+        total = total + column_in[d].astype(jnp.float32)
+    moe_ref[...] = total.astype(jnp.bfloat16)
+    for copy in started:
+        copy.wait_send()
+
+
+def reduce_blocks(part, heads, gain):
+    experts, parts, rows, width = part.shape
+    depth = experts // 2
+    vmem = pl.BlockSpec(memory_space=pltpu.VMEM)
+    block = (rows, width)
+    held = lambda *lead: pltpu.VMEM(lead + block, jnp.bfloat16)
+    sems = lambda *shape: pltpu.SemaphoreType.DMA(shape)
+    return pl.pallas_call(
+        functools.partial(reduce_kernel, depth),
+        out_shape=[jax.ShapeDtypeStruct(block, jnp.bfloat16)] * 2,
+        in_specs=[vmem] * 3,
+        out_specs=[vmem] * 2,
+        scratch_shapes=[
+            held(depth, 2, 2), held(depth, 2, 2), held(depth), held(depth), held(depth), held(depth),
+            held(), held(2), held(),
+            sems(3 + 4 * depth + 3 * depth + depth - 1), sems(depth, 2, 2), sems(3, depth),
+            sems(depth), sems(3),
+        ],
+        compiler_params=pltpu.CompilerParams(
+            collective_id=1, has_side_effects=True, vmem_limit_bytes=48 * 1024 * 1024
+        ),
+        name="reduce_blocks",
+    )(part, heads, gain.reshape(1, -1))
+
+
+def dense_local(
+    mix_in, mix_gain, query_weight, latent_weight, rotary_weight, latent_gain, key_weight,
+    value_weight, output_weight, out_gain, ffn_in, ffn_gain, gate_weight, up_weight, down_weight,
+    routes, route_scores,
+):
+    f32, bf16 = jnp.float32, jnp.bfloat16
+    experts, parts = lax.axis_size("ep"), lax.axis_size("tp")
+    ep, tp = lax.axis_index("ep"), lax.axis_index("tp")
+    row_count, width = mix_in.shape
+    quarter = row_count // parts
+    latent_width = latent_weight.shape[1]
+    half = ROPE // 2
+    first_row = ep * row_count
+
+    def own(array):
+        return lax.dynamic_slice_in_dim(array, tp * quarter, quarter, 0)
+
+    rows = rms_rows(own(ffn_in).astype(f32), ffn_gain).astype(bf16)
+    own_normed = rms_rows(own(mix_in).astype(f32), mix_gain).astype(bf16)
+    latent = rms_rows(jnp.dot(own_normed, latent_weight, preferred_element_type=f32), latent_gain)
+    turned = jnp.dot(own_normed, rotary_weight, preferred_element_type=f32)
+    positions = first_row + jnp.arange(row_count, dtype=jnp.int32)
+    inverse = rope_base ** (-jnp.arange(0, ROPE, 2).astype(f32) / ROPE)
+    angles = positions.astype(f32)[:, None] * inverse[None, :]
+    cosine, sine = jnp.cos(angles), jnp.sin(angles)
+
+    def rotate(vectors, cosine, sine):
+        upper, lower = vectors[..., :half], vectors[..., half:]
+        return jnp.concatenate([upper * cosine - lower * sine, lower * cosine + upper * sine], axis=-1)
+
+    rotary_key = rotate(turned, own(cosine), own(sine))
+    shares = jax.nn.softmax(own(route_scores), axis=-1)
+    named = own(routes)[:, :, None] == jnp.arange(experts, dtype=jnp.int32)[None, None, :]
+    table = jnp.sum(jnp.where(named, shares[:, :, None], 0.0), axis=1)
+    coarse = lax.reduce_precision(table, 8, 7)
+    used = latent_width + ROPE + 2 * experts
+    side_width = -(-used // 128) * 128
+    side = jnp.concatenate(
+        [latent, rotary_key, coarse, table - coarse, jnp.zeros((quarter, side_width - used), f32)],
+        axis=1,
+    ).astype(bf16)
+    all_rows, all_side = gather_blocks(rows, side, experts, parts)
+    tokens = experts * row_count
+    all_rows = all_rows.reshape(tokens, width)
+    all_side = all_side.reshape(tokens, side_width)
+
+    split = latent_width + ROPE
+    share_columns = all_side[:, split : split + 2 * experts].astype(f32)
+    share_table = share_columns[:, :experts] + share_columns[:, experts:]
+    is_mine = (jnp.arange(experts, dtype=jnp.int32) == ep)[None, :]
+    share = jnp.sum(jnp.where(is_mine, share_table, 0.0), axis=1, keepdims=True)
+    gate_part = jnp.dot(all_rows, gate_weight[0], preferred_element_type=f32)
+    up_part = jnp.dot(all_rows, up_weight[0], preferred_element_type=f32)
+    hidden = clamped_unit(gate_part, up_part).astype(bf16)
+    part = (jnp.dot(hidden, down_weight[0], preferred_element_type=f32) * share).astype(bf16)
+
+    normed = rms_rows(mix_in.astype(f32), mix_gain).astype(bf16)
+    head_count = query_weight.shape[1] // (NOPE + ROPE)
+    queries = jnp.dot(normed, query_weight, preferred_element_type=f32).reshape(
+        row_count, head_count, NOPE + ROPE
+    )
+    query_plain = queries[..., :NOPE].astype(bf16)
+    query_turn = rotate(queries[..., NOPE:], cosine[:, None, :], sine[:, None, :]).astype(bf16)
+    all_latent = all_side[:, :latent_width]
+    all_turned = all_side[:, latent_width:split]
+    across = (((0,), (1,)), ((), ()))
+    keys = lax.dot_general(key_weight, all_latent, across, preferred_element_type=f32).astype(bf16)
+    values = lax.dot_general(value_weight, all_latent, across, preferred_element_type=f32).astype(bf16)
+    keys = keys.reshape(head_count, NOPE, tokens)
+    values = values.reshape(head_count, VD, tokens)
+    scores = jnp.einsum("ihd,hdj->hij", query_plain, keys, preferred_element_type=f32)
+    scores = scores + jnp.einsum("ihd,jd->hij", query_turn, all_turned, preferred_element_type=f32)
+    allowed = jnp.arange(tokens, dtype=jnp.int32)[None, :] <= positions[:, None]
+    weights = jnp.where(allowed[None], jnp.exp(scores * (NOPE + ROPE) ** (-0.5)), 0.0)
+    totals = jnp.sum(weights, axis=-1)
+    weighted = jnp.einsum("hij,hdj->hid", weights.astype(bf16), values, preferred_element_type=f32)
+    attended = (weighted / totals[..., None]).astype(bf16)
+    mixing = output_weight.reshape(head_count, VD, width)
+    heads = jnp.einsum("hid,hde->ie", attended, mixing, preferred_element_type=f32).astype(bf16)
+    mixed, moe_out = reduce_blocks(
+        part.reshape(experts, parts, quarter, width), heads.reshape(parts, quarter, width), out_gain
+    )
+    return mixed, moe_out
+
+
 def solution(mesh):
+    experts, parts = mesh.shape["ep"], mesh.shape["tp"]
+
+    def body(*args):
+        quarter, choose = args[10].shape[0] // parts, args[15].shape[1]
+        every_row = 2 * quarter * choose >= quarter * experts
+        paired = parts == 4 and experts % 2 == 0 and (experts // 2) & (experts // 2 - 1) == 0
+        return (dense_local if every_row and paired else local)(*args)
     placed = (
         P("ep", None),
         P(),
@@ -235,7 +560,7 @@
         P("ep", None),
     )
     return jax.shard_map(
-        local,
+        body,
         mesh=mesh,
         in_specs=placed,
         out_specs=(P(("ep", "tp"), None), P(("ep", "tp"), None)),

time: 234 us -> 123 us (0.53)
  waiting for transfers between devices: 81.7 us -> 0 us
  Pallas kernels: 0 us -> 71.6 us
  blocking collectives: 60.5 us -> 0 us
  local copies, waits for them, and re-layouts: 26.4 us -> 8.6 us
  between operations: 14 us -> 0.89 us
  starting transfers between devices: 5.68 us -> 0 us
  other arithmetic: 13.9 us -> 9.19 us
    pallas_call x0 -> x2, Pallas kernels: none -> 71.6 us  [the longest x1 38 us: gather_blocks(): pl.pallas_call(functools.partial(gather_kernel, depth), out_shape=whole,...]
    reduce_scatter x2 -> x0, waiting for transfers between devices: 45.1 us -> none  [local(): lax.psum_scatter(lax.optimization_barrier(partial_value.astype(jnp.bfloat...]
    all_to_all x1 -> x0, blocking collectives: 32.8 us -> none  [local(): lax.all_to_all(outgoing, 'ep', split_axis=1, concat_axis=1, tiled=True)]
    all_gather x2 -> x0, waiting for transfers between devices: 29.2 us -> none  [the longest x1 29.2 us: local(): row_block = lax.all_gather(arrived, 'tp', axis=0, tiled=True)]
    all_gather x1 -> x0, blocking collectives: 27.7 us -> none  [local(): lax.all_gather(rotary_key, 'ep', axis=1, tiled=True)]
    gather x2 -> x0, local copies, waits for them, and re-layouts: 8.07 us -> none  [the longest x1 4.48 us: local(): outgoing = padded[chosen].reshape(capacity, experts, -1)]
    all_to_all x1 -> x0, waiting for transfers between devices: 7.37 us -> none  [local(): lax.all_to_all(result, 'ep', split_axis=1, concat_axis=1, tiled=True)]
    all_to_all x1 -> x0, starting transfers between devices: 5.52 us -> none  [local(): lax.all_to_all(result, 'ep', split_axis=1, concat_axis=1, tiled=True)]
  transfers between devices with their start and end apart: 5 -> 0, of which waited for: 4 -> 0; matrix products, arithmetic and copies ran while one was open for 18% -> 0% of each run, Pallas kernels for 0% -> 0%
where the time goes in v1:
time: 123 us
  Pallas kernels  71.6 us (58%)
  matrix products  32.2 us (26%)
  other arithmetic  9.19 us (7%)
  local copies, waits for them, and re-layouts  8.6 us (7%)
    pallas_call x1, Pallas kernels, gather_blocks(): pl.pallas_call(functools.partial(gather_kernel, depth), out_shape=whole,...  38 us
    pallas_call x1, Pallas kernels, reduce_blocks(): pl.pallas_call(functools.partial(reduce_kernel, depth), out_shape=[jax.Sh...  33.6 us
    dot_general x1, matrix products, dense_local(): jnp.dot(hidden, down_weight[0], preferred_element_type=f32) * share  9.49 us
    unnamed x32, local copies, waits for them, and re-layouts  5.15 us
    dot_general x1, matrix products, dense_local(): gate_part = jnp.dot(all_rows, gate_weight[0], preferred_element_type=f32)  4.81 us
    dot_general x1, matrix products, dense_local(): jnp.einsum('hid,hde->ie', attended, mixing, preferred_element_type=f32)  3.82 us
    dot_general x1, matrix products, dense_local(): jnp.einsum('ihd,jd->hij', query_turn, all_turned, preferred_element_type=...  3.5 us

profile of v1, /device:TPU:0, one launch (start us, length us, event | category | flops | bytes accessed | tf_op | source)
XLA Modules:
  0.0 122.5 jit_solution(11126090234329342215)
XLA Ops:
  0.6 0.0 copy-start
  0.6 0.0 copy-start.11
  0.7 0.0 copy-start.13
  0.7 0.0 copy-start.10
  0.7 0.0 copy-start.12
  0.7 0.9 fusion.54
  1.6 0.9 fusion.51
  2.5 0.8 fusion.50
  3.3 0.8 constant_dynamic-slice_fusion.1
  4.0 0.1 copy.45
  4.1 0.1 copy.46
  4.2 1.1 fusion.35
  5.3 2.3 %multiply_reduce_fusion = (f32[32]{0:T(128)S(1)}, f32[32,512]{1,0:T(8,128)S(1)}) fusion(bf16[2048,512]{1,0:T(8,128)(2,1)} %param.20, f32[2048]{0:T(1024)} %param.18, f32[32]{0:T(128)S(1)} %add_rsqrt_fusion.2, bf16[128,2048]{1,0:T(8,128)(2,1)} %param.17, s32[]{:T(128)S(6)} %select_n.20), kind=kOutput, calls=%fused_computation.67 | convolution fusion | flops 67403744 | bytes 2302212 | tf_op jit(solution)/shard_map/dot_general | solution.py:469
  7.7 0.0 copy-done.13
  7.7 0.1 multiply_convert_fusion.1
  7.8 0.0 copy-done.11
  7.8 0.0 copy-done.10
  7.8 1.2 fusion.46
  8.9 0.6 iota_add_fusion
  9.5 0.3 multiply_cosine_fusion
  9.9 0.0 copy-start.8
  9.9 0.0 copy-start.9
  9.9 0.1 add_convert_fusion.1
  10.0 0.5 copy-done.8
  10.5 0.0 copy-done.9
  10.5 0.1 concatenate.8.side_ref
  10.6 0.0 copy-start.7
  10.6 0.0 copy-done.12
  10.6 1.1 fusion.37.row_ref
  11.7 38.0 %gather_blocks.1 = (bf16[8,4,32,2048]{3,2,1,0:T(8,128)(2,1)S(1)}, bf16[8,4,32,640]{3,2,1,0:T(8,128)(2,1)S(1)}) custom-call(bf16[32,2048]{1,0:T(8,128)(2,1)S(1)} %fusion.37.row_ref, bf16[32,640]{1,0:T(8,128)(2,1)S(1)} %concatenate.8.side_ref), custom_call_target="tpu_custom_call" | custom-call | tf_op jit(solution)/shard_map/gather_blocks/pallas_call | solution.py:323
  49.7 0.0 copy-start.3
  49.7 0.0 copy-start.6
  49.7 2.2 %convolution_convert_fusion.1 = bf16[1024,512]{0,1:T(8,128)(2,1)S(1)} fusion(bf16[512,512]{1,0:T(8,128)(2,1)} %param.23, bf16[1024,640]{1,0:T(8,128)(2,1)S(1)} %bitcast.54), kind=kOutput, calls=%fused_computation.8 | convolution fusion | flops 537395200 | bytes 2621440 | tf_op jit(solution)/shard_map/dot_general | solution.py:516
  51.9 0.0 copy-done.7
  51.9 0.2 fusion.8
  52.1 0.0 copy-done
  52.2 1.4 %fusion.25 = f32[128,768]{0,1:T(8,128)S(1)} fusion(bf16[2048,768]{1,0:T(8,128)(2,1)S(1)} %copy-done, bf16[128,2048]{1,0:T(8,128)(2,1)S(1)} %copy-done.7, f32[2048]{0:T(1024)S(1)} %copy-done.11, f32[128]{0:T(128)S(1)} %add_rsqrt_fusion), kind=kOutput, calls=%fused_computation.33 | convolution fusion | flops 403701760 | bytes 4071936 | tf_op jit(solution)/shard_map/dot_general | solution.py:508
  53.5 0.0 copy-done.3
  53.5 0.0 copy-done.6
  53.6 1.8 %fusion.41 = f32[4,128,1024]{2,1,0:T(8,128)} fusion(bf16[4,128,1024]{2,1,0:T(8,128)(2,1)S(1)} %bitcast.63, f32[128,4,192]{0,2,1:T(8,128)S(1)} %bitcast.61), kind=kOutput, calls=%fused_computation.57 | convolution fusion | flops 134217728 | bytes 3276800 | tf_op jit(solution)/shard_map/ihd,hdj->hij/dot_general | solution.py:520
  55.4 0.9 copy.51
  56.3 1.5 %copy.52 = f32[128,32]{0,1:T(8,128)} copy(f32[128,32]{1,0:T(8,128)} %copy-done.8) | data formatting | bytes 32768 | tf_op jit(solution)/shard_map/sin | solution.py:474
  57.8 0.0 copy-start.4
  57.8 0.0 copy-start.14
  57.8 0.9 subtract_convert_fusion
  58.7 0.8 iota_compare_fusion
  59.5 3.5 %fusion.61 = (f32[4,128]{1,0:T(4,128)S(1)}, bf16[4,128,1024]{2,1,0:T(8,128)(2,1)}) fusion(f32[4,128,1024]{2,1,0:T(8,128)} %fusion.41, bf16[128,4,32]{0,2,1:T(8,128)(2,1)S(1)} %get-tuple-element.7, bf16[128,4,32]{0,2,1:T(8,128)(2,1)S(1)} %get-tuple-element.6, bf16[1024,640]{1,0:T(8,128)(2,1)} %bitcast.55, pred[128,1024]{1,0:T(8,128)(4,1)S(1)} %iota_compare_fusion), kind=kOutput, calls=%fused_computation.96 | convolution fusion | flops 69860864 | bytes 3606528 | tf_op jit(solution)/shard_map/ihd,jd->hij/dot_general | solution.py:521
  63.0 0.0 copy-done.4
  63.0 0.0 copy-done.14
  63.0 1.7 %convolution_convert_fusion = bf16[1024,512]{0,1:T(8,128)(2,1)} fusion(bf16[512,512]{1,0:T(8,128)(2,1)S(1)} %copy-done.14, bf16[1024,640]{1,0:T(8,128)(2,1)S(1)} %bitcast.57), kind=kOutput, calls=%fused_computation.7 | convolution fusion | flops 537395200 | bytes 2621440 | tf_op jit(solution)/shard_map/dot_general | solution.py:517
  64.7 3.8 %fusion = bf16[128,2048]{1,0:T(8,128)(2,1)} fusion(bf16[4,128,2048]{2,1,0:T(8,128)(2,1)} %bitcast.64, bf16[4,128,1024]{2,1,0:T(8,128)(2,1)} %bitcast.65, bf16[4,128,1024]{2,1,0:T(8,128)(2,1)} %get-tuple-element.17, f32[4,128]{1,0:T(4,128)S(1)} %get-tuple-element.16), kind=kOutput, calls=%fused_computation.2 | convolution fusion | flops 403046400 | bytes 4720640 | tf_op jit(solution)/shard_map/hid,hde->ie/dot_general | solution.py:528
  68.6 4.8 %convolution_minimum_fusion = f32[1024,256]{1,0:T(8,128)} fusion(bf16[1024,2048]{1,0:T(8,128)(2,1)} %bitcast.59, bf16[1,2048,256]{2,1,0:T(8,128)(2,1)} %param.29), kind=kOutput, calls=%fused_computation.9 | convolution fusion | flops 1074003968 | bytes 6291456 | tf_op jit(solution)/shard_map/dot_general | solution.py:501
  73.4 1.1 slice_convert_fusion.1
  74.5 0.4 fusion.28
  74.8 0.0 copy-start.5
  74.8 9.5 %multiply_convert_fusion = bf16[1024,2048]{1,0:T(8,128)(2,1)} fusion(f32[1024]{0:T(1024)S(1)} %fusion.28, bf16[1024,2048]{1,0:T(8,128)(2,1)} %bitcast.60, bf16[1,256,2048]{2,1,0:T(8,128)(2,1)} %param.31, bf16[1,2048,256]{2,1,0:T(8,128)(2,1)} %param.30, f32[1024,256]{1,0:T(8,128)} %convolution_minimum_fusion), kind=kOutput, calls=%fused_computation | convolution fusion | flops 2154037248 | bytes 11538432 | tf_op jit(solution)/shard_map/dot_general | solution.py:504
  84.3 0.0 copy-done.5
  84.3 0.0 copy-start.1
  84.3 2.2 %copy-done.1 = bf16[1024,2048]{1,0:T(8,128)(2,1)S(1)} copy-done((bf16[1024,2048]{1,0:T(8,128)(2,1)S(1)}, bf16[1024,2048]{1,0:T(8,128)(2,1)}, u32[]{:S(2)}) %copy-start.1) | copy-done | bytes 4194328
  86.5 0.0 copy-start.2
  86.5 1.0 copy-done.2
  87.6 33.6 %reduce_blocks.1 = (bf16[32,2048]{1,0:T(8,128)(2,1)S(1)}, bf16[32,2048]{1,0:T(8,128)(2,1)S(1)}) custom-call(bf16[8,4,32,2048]{3,2,1,0:T(8,128)(2,1)S(1)} %bitcast.52, bf16[4,32,2048]{2,1,0:T(8,128)(2,1)S(1)} %bitcast.53, f32[1,2048]{1,0:T(1,128)S(1)} %bitcast.58), custom_call_target="tpu_custom_call" | custom-call | tf_op jit(solution)/shard_map/reduce_blocks/pallas_call | solution.py:432
  121.2 0.7 copy.60
  121.9 0.7 copy.61
  (10 shorter events, 0.1 us)
Async XLA Ops:
  0.6 51.5 %copy-start = (bf16[2048,768]{1,0:T(8,128)(2,1)S(1)}, bf16[2048,768]{1,0:T(8,128)(2,1)}, u32[]{:S(2)}) copy-start(bf16[2048,768]{1,0:T(8,128)(2,1)} %param.19) | copy-start | bytes 9437188
  0.6 7.1 %copy-start.11 = (f32[2048]{0:T(1024)S(1)}, f32[2048]{0:T(1024)}, u32[]{:S(2)}) copy-start(f32[2048]{0:T(1024)} %param.18) | copy-start | bytes 24580
  0.7 7.0 %copy-start.13 = (f32[512]{0:T(512)S(1)}, f32[512]{0:T(512)}, u32[]{:S(2)}) copy-start(f32[512]{0:T(512)} %param.22) | copy-start | bytes 6148
  0.7 7.1 %copy-start.10 = (bf16[2048,64]{0,1:T(8,128)(2,1)S(1)}, bf16[2048,64]{0,1:T(8,128)(2,1)}, u32[]{:S(2)}) copy-start(bf16[2048,64]{0,1:T(8,128)(2,1)} %param.21) | copy-start | bytes 786436
  0.7 10.0 %copy-start.12 = (f32[2048]{0:T(1024)S(1)}, f32[2048]{0:T(1024)}, u32[]{:S(2)}) copy-start(f32[2048]{0:T(1024)} %param.28) | copy-start | bytes 24580
  9.9 0.6 copy-start.8
  9.9 0.6 copy-start.9
  10.6 41.3 %copy-start.7 = (bf16[128,2048]{1,0:T(8,128)(2,1)S(1)}, bf16[128,2048]{1,0:T(8,128)(2,1)}, u32[]{:S(2)}) copy-start(bf16[128,2048]{1,0:T(8,128)(2,1)} %param.17) | copy-start | bytes 1572868
  49.7 3.8 %copy-start.3 = (bf16[8,4,32,640]{3,2,1,0:T(8,128)(2,1)}, bf16[8,4,32,640]{3,2,1,0:T(8,128)(2,1)S(1)}, u32[]{:S(2)}) copy-start(bf16[8,4,32,640]{3,2,1,0:T(8,128)(2,1)S(1)} %get-tuple-element.5) | copy-start | bytes 3932164
  49.7 3.8 %copy-start.6 = (bf16[8,4,32,2048]{3,2,1,0:T(8,128)(2,1)}, bf16[8,4,32,2048]{3,2,1,0:T(8,128)(2,1)S(1)}, u32[]{:S(2)}) copy-start(bf16[8,4,32,2048]{3,2,1,0:T(8,128)(2,1)S(1)} %get-tuple-element.4) | copy-start | bytes 12582916
  57.8 5.2 %copy-start.4 = (bf16[8,4,32,640]{3,2,1,0:T(8,128)(2,1)S(1)}, bf16[8,4,32,640]{3,2,1,0:T(8,128)(2,1)}, u32[]{:S(2)}) copy-start(bf16[8,4,32,640]{3,2,1,0:T(8,128)(2,1)} %copy-done.3) | copy-start | bytes 3932164
  57.8 5.2 %copy-start.14 = (bf16[512,512]{1,0:T(8,128)(2,1)S(1)}, bf16[512,512]{1,0:T(8,128)(2,1)}, u32[]{:S(2)}) copy-start(bf16[512,512]{1,0:T(8,128)(2,1)} %param.24) | copy-start | bytes 1572868
  74.8 9.5 %copy-start.5 = (f32[2048]{0:T(1024)S(1)}, f32[2048]{0:T(1024)}, u32[]{:S(2)}) copy-start(f32[2048]{0:T(1024)} %param.26) | copy-start | bytes 24580
  84.3 2.2 %copy-start.1 = (bf16[1024,2048]{1,0:T(8,128)(2,1)S(1)}, bf16[1024,2048]{1,0:T(8,128)(2,1)}, u32[]{:S(2)}) copy-start(bf16[1024,2048]{1,0:T(8,128)(2,1)} %multiply_convert_fusion) | copy-start | bytes 12582916
  86.5 1.0 copy-start.2

commit v2 on v0

--- a/solution.py
+++ b/solution.py
@@ -1,6 +1,9 @@
 import jax
 import jax.numpy as jnp
+import functools
 from jax import lax
+from jax.experimental import pallas as pl
+from jax.experimental.pallas import tpu as pltpu
 from jax.sharding import PartitionSpec as P
 
 NOPE = 128
@@ -214,7 +217,386 @@
     return (mixed, moe_out)
 
 
+MESH = pl.DeviceIdType.MESH
+
+
+def flip(value, bits):
+    bit = 1
+    while bit <= bits:
+        if bits & bit:
+            value = value + bit - 2 * bit * ((value // bit) % 2)
+        bit *= 2
+    return value
+
+
+def here():
+    ep, tp = lax.axis_index("ep"), lax.axis_index("tp")
+    return ep // 2, ep % 2, tp // 2, tp % 2
+
+
+def place(z, x, y, core):
+    return {"ep": z * 2 + x, "tp": y * 2 + core}
+
+
+def greet(partners):
+    barrier = pltpu.get_barrier_semaphore()
+    for partner in partners:
+        pl.semaphore_signal(barrier, inc=1, device_id=partner, device_id_type=MESH)
+    pl.semaphore_wait(barrier, len(partners))
+
+
+def layer_kernel(
+    depth, heads, row_ref, side_ref, query_ref, gain_ref, gate_hbm, up_hbm, down_hbm, key_hbm,
+    value_hbm, output_hbm, mixed_ref, moe_ref,
+    rows_all, side_all, part_ref, work, twin_in, hop_in, direct_in, relay_in, column_in,
+    heads_ref, heads_work, heads_twin, heads_in, keys, values, attended, own_total,
+    gate_ref, up_ref, down_ref, key_ref, value_ref, output_ref,
+    spread_sem, recv_sem, send_sem, twin_sem, square_sem, column_sem, heads_sem, load_sem,
+):
+    f32, bf16 = jnp.float32, jnp.bfloat16
+    ep = lax.axis_index("ep")
+    z, x, y, core = here()
+    x_next, y_next, twin = place(z, 1 - x, y, core), place(z, x, 1 - y, core), place(z, x, y, 1 - core)
+    columns = [place(flip(z, d), x, y, core) for d in range(1, depth)]
+    parts, quarter, width = part_ref.shape[1:]
+    row_count = parts * quarter
+    side_width = side_ref.shape[1]
+    latent_width = key_ref.shape[0]
+    experts = 2 * depth
+    loads = [
+        pltpu.make_async_copy(src, dst, load_sem.at[n])
+        for n, (src, dst) in enumerate(
+            (
+                (gate_hbm, gate_ref), (up_hbm, up_ref), (down_hbm, down_ref),
+                (key_hbm, key_ref), (value_hbm, value_ref), (output_hbm, output_ref),
+            )
+        )
+    ]
+    for load in loads:
+        load.start()
+    greet(columns + [x_next, y_next, twin])
+    spread, started = [], []
+
+    def copies(origin, target, own):
+        e, t = origin["ep"], origin["tp"]
+        number = len(spread)
+        return [
+            pltpu.make_async_remote_copy(
+                src_ref=held if own else out.at[e, t],
+                dst_ref=out.at[e, t],
+                send_sem=spread_sem.at[a, number],
+                recv_sem=recv_sem.at[a, e, t],
+                device_id=target,
+                device_id_type=MESH,
+            )
+            for a, (held, out) in enumerate(((side_ref, side_all), (row_ref, rows_all)))
+        ]
+
+    def give(origin, target, own=False):
+        pair = copies(origin, target, own)
+        for copy in pair:
+            copy.start()
+        spread.append(pair)
+
+    def take(origin):
+        for copy in copies(origin, twin, False):
+            copy.wait_recv()
+
+    def make(src, dst, sem, target):
+        return pltpu.make_async_remote_copy(
+            src_ref=src, dst_ref=dst, send_sem=send_sem.at[len(started)], recv_sem=sem,
+            device_id=target, device_id_type=MESH,
+        )
+
+    def send(src, dst, sem, target):
+        copy = make(src, dst, sem, target)
+        copy.start()
+        started.append(copy)
+
+    def arrive(dst, sem):
+        make(dst, dst, sem, twin).wait_recv()
+
+    def forward_column(d):
+        origin = place(flip(z, d), x, y, core)
+        take(origin)
+        for target in (x_next, y_next, twin):
+            give(origin, target)
+
+    def forward_square(d):
+        at = flip(z, d)
+        from_x, from_y = place(at, 1 - x, y, core), place(at, x, 1 - y, core)
+        take(from_x)
+        if d % 2 == 0:
+            give(from_x, y_next)
+        give(from_x, twin)
+        take(from_y)
+        if d % 2 == 1:
+            give(from_y, x_next)
+        give(from_y, twin)
+
+    def forward_corner(d):
+        origin = place(flip(z, d), 1 - x, 1 - y, core)
+        take(origin)
+        give(origin, twin)
+
+    def side_block(e):
+        return side_all[e].reshape(row_count, side_width)
+
+    lane = lax.broadcasted_iota(jnp.int32, (row_count, side_width - latent_width), 1)
+    is_mine = (lane == ROPE + ep) | (lane == ROPE + experts + ep)
+
+    def expert_plane(d):
+        for a in (0, 1):
+            for b in (0, 1):
+                take(place(flip(z, d), flip(x, a), flip(y, b), 1 - core))
+
+        @pl.loop(0, 2)
+        def _(i):
+            e = flip(z, d) * 2 + i
+            block = rows_all[e].reshape(row_count, width)
+            gate_part = jnp.dot(block, gate_ref[...], preferred_element_type=f32)
+            up_part = jnp.dot(block, up_ref[...], preferred_element_type=f32)
+            hidden = clamped_unit(gate_part, up_part).astype(bf16)
+            table = side_block(e)[:, latent_width:].astype(f32)
+            share = jnp.sum(jnp.where(is_mine, table, 0.0), axis=1, keepdims=True)
+            chunk = 512
+            for n in range(0, width, chunk):
+                piece = jnp.dot(hidden, down_ref[:, n : n + chunk], preferred_element_type=f32) * share
+                part_ref[e, :, :, n : n + chunk] = piece.astype(bf16).reshape(parts, quarter, chunk)
+
+        for a, b in ((1, 1), (1, 0), (0, 1), (0, 0)):
+            e, t = flip(z, d) * 2 + flip(x, a), flip(y, b) * 2 + 1 - core
+            send(part_ref.at[e, t], twin_in.at[d, a, b], twin_sem.at[d, a, b], twin)
+
+    def paired(d, a, b):
+        arrive(twin_in.at[d, a, b], twin_sem.at[d, a, b])
+        own = part_ref[flip(z, d) * 2 + flip(x, a), flip(y, b) * 2 + core]
+        return own.astype(f32) + twin_in[d, a, b].astype(f32)
+
+    def sum_pairs(d):
+        work[d, 1, 1] = paired(d, 1, 1).astype(bf16)
+        send(work.at[d, 1, 1], hop_in.at[d], square_sem.at[0, d], y_next if d % 2 else x_next)
+        a, b = (0, 1) if d % 2 else (1, 0)
+        work[d, a, b] = paired(d, a, b).astype(bf16)
+        send(work.at[d, a, b], direct_in.at[d], square_sem.at[1, d], y_next if d % 2 else x_next)
+
+    def sum_relay(d):
+        a, b = (1, 0) if d % 2 else (0, 1)
+        value = paired(d, a, b)
+        arrive(hop_in.at[d], square_sem.at[0, d])
+        work[d, a, b] = (value + hop_in[d].astype(f32)).astype(bf16)
+        send(work.at[d, a, b], relay_in.at[d], square_sem.at[2, d], x_next if d % 2 else y_next)
+
+    def sum_square(d):
+        value = paired(d, 0, 0)
+        arrive(direct_in.at[d], square_sem.at[1, d])
+        value = value + direct_in[d].astype(f32)
+        arrive(relay_in.at[d], square_sem.at[2, d])
+        value = value + relay_in[d].astype(f32)
+        if d:
+            work[d, 0, 0] = value.astype(bf16)
+            send(work.at[d, 0, 0], column_in.at[d], column_sem.at[d], columns[d - 1])
+        else:
+            own_total[...] = value
+
+    across = (((1,), (1,)), ((), ()))
+    score_scale = (NOPE + ROPE) ** (-0.5)
+
+    def expand():
+        @pl.loop(0, experts)
+        def _(e):
+            block = side_block(e)
+            latent, rest = block[:, :latent_width], block[:, latent_width:]
+            at = pl.ds(pl.multiple_of(e * row_count, row_count), row_count)
+            key_block = jnp.dot(latent, key_ref[...], preferred_element_type=f32).astype(bf16)
+            value_block = jnp.dot(latent, value_ref[...], preferred_element_type=f32).astype(bf16)
+            for h in range(heads):
+                keys[h, at, :NOPE] = key_block[:, h * NOPE : (h + 1) * NOPE]
+                keys[h, at, NOPE:] = rest
+                values[h, at, :] = value_block[:, h * VD : (h + 1) * VD]
+
+    def attend(h):
+        tokens = experts * row_count
+        chunk = 256
+        totals = jnp.zeros((row_count, 1), f32)
+        weighted = jnp.zeros((row_count, VD), f32)
+        places = lax.broadcasted_iota(jnp.int32, (row_count, chunk), 0) + ep * row_count
+        for n in range(0, tokens, chunk):
+            scores = lax.dot_general(
+                query_ref[h], keys[h, n : n + chunk, :], across, preferred_element_type=f32
+            )
+            allowed = lax.broadcasted_iota(jnp.int32, (row_count, chunk), 1) + n <= places
+            weights = jnp.where(allowed, jnp.exp(scores * score_scale), 0.0)
+            totals = totals + jnp.sum(weights, axis=1, keepdims=True)
+            weighted = weighted + jnp.dot(
+                weights.astype(bf16), values[h, n : n + chunk, :], preferred_element_type=f32
+            )
+        attended[:, h * VD : (h + 1) * VD] = (weighted / totals).astype(bf16)
+
+    def project():
+        chunk = 512
+        for n in range(0, width, chunk):
+            piece = jnp.dot(attended[...], output_ref[:, n : n + chunk], preferred_element_type=f32)
+            heads_ref[:, :, n : n + chunk] = piece.astype(bf16).reshape(parts, quarter, chunk)
+        for b in (1, 0):
+            send(heads_ref.at[flip(y, b) * 2 + 1 - core], heads_twin.at[b], heads_sem.at[b], twin)
+
+    me = place(z, x, y, core)
+    for target in columns + [x_next, y_next, twin]:
+        give(me, target, True)
+    rows_all[me["ep"], me["tp"]] = row_ref[...]
+    side_all[me["ep"], me["tp"]] = side_ref[...]
+    for load in loads:
+        load.wait()
+
+    def reduce_after(last):
+        for step, back in ((sum_pairs, 0), (sum_relay, 1), (sum_square, 2)):
+            if 0 <= last - back < depth:
+                step(last - back)
+
+    for d in range(1, depth + 3):
+        if d < depth:
+            forward_column(d)
+        if d - 1 < depth:
+            forward_square(d - 1)
+        if 0 <= d - 2 < depth:
+            forward_corner(d - 2)
+        if 0 <= d - 3 < depth:
+            expert_plane(d - 3)
+        if 0 <= d - 4:
+            reduce_after(d - 4)
+    expand()
+    reduce_after(depth - 1)
+    for h in range(heads):
+        attend(h)
+        if h % 2 == 0 and h < 4:
+            reduce_after(depth + h // 2)
+    for h in range((heads + 1) // 2, 2):
+        reduce_after(depth + h)
+    project()
+    arrive(heads_twin.at[1], heads_sem.at[1])
+    heads_work[...] = (
+        heads_ref[(1 - y) * 2 + core].astype(f32) + heads_twin[1].astype(f32)
+    ).astype(bf16)
+    send(heads_work, heads_in, heads_sem.at[2], y_next)
+    total = own_total[...]
+    for d in range(1, depth):
+        arrive(column_in.at[d], column_sem.at[d])
+        total = total + column_in[d].astype(f32)
+    moe_ref[...] = total.astype(bf16)
+    arrive(heads_twin.at[0], heads_sem.at[0])
+    arrive(heads_in, heads_sem.at[2])
+    projected = (
+        heads_ref[y * 2 + core].astype(f32) + heads_twin[0].astype(f32) + heads_in[...].astype(f32)
+    )
+    mixed_ref[...] = rms_rows(projected, gain_ref[...]).astype(bf16)
+    for copy in started:
+        copy.wait_send()
+    for pair in spread:
+        for copy in pair:
+            copy.wait_send()
+
+
+def layer(rows, side, queries, gain, weights, experts, parts):
+    depth, heads = experts // 2, queries.shape[0]
+    quarter, width = rows.shape
+    row_count = quarter * parts
+    tokens = experts * row_count
+    vmem, anywhere = pl.BlockSpec(memory_space=pltpu.VMEM), pl.BlockSpec(memory_space=pl.ANY)
+    held = lambda *lead: pltpu.VMEM(lead + (quarter, width), jnp.bfloat16)
+    scratch = lambda *shape: pltpu.VMEM(shape, jnp.bfloat16)
+    sems = lambda *shape: pltpu.SemaphoreType.DMA(shape)
+    gives = depth + 2 + 3 * (depth - 1) + 3 * depth + depth
+    return pl.pallas_call(
+        functools.partial(layer_kernel, depth, heads),
+        out_shape=[jax.ShapeDtypeStruct((quarter, width), jnp.bfloat16)] * 2,
+        in_specs=[vmem] * 4 + [anywhere] * len(weights),
+        out_specs=[vmem] * 2,
+        scratch_shapes=[
+            held(experts, parts), scratch(experts, parts, quarter, side.shape[1]),
+            held(experts, parts), held(depth, 2, 2), held(depth, 2, 2),
+            held(depth), held(depth), held(depth), held(depth),
+            held(parts), held(), held(2), held(),
+            scratch(heads, tokens, queries.shape[2]), scratch(heads, tokens, VD),
+            scratch(row_count, heads * VD), pltpu.VMEM((quarter, width), jnp.float32),
+        ]
+        + [scratch(*w.shape) for w in weights]
+        + [
+            sems(2, gives + 1), sems(2, experts, parts), sems(3 + 8 * depth), sems(depth, 2, 2),
+            sems(3, depth), sems(depth), sems(3), sems(len(weights)),
+        ],
+        compiler_params=pltpu.CompilerParams(
+            collective_id=0, has_side_effects=True, vmem_limit_bytes=56 * 1024 * 1024
+        ),
+        name="layer",
+    )(rows, side, queries, gain.reshape(1, -1), *weights)
+
+
+def dense_local(
+    mix_in, mix_gain, query_weight, latent_weight, rotary_weight, latent_gain, key_weight,
+    value_weight, output_weight, out_gain, ffn_in, ffn_gain, gate_weight, up_weight, down_weight,
+    routes, route_scores,
+):
+    f32, bf16 = jnp.float32, jnp.bfloat16
+    experts, parts = lax.axis_size("ep"), lax.axis_size("tp")
+    ep, tp = lax.axis_index("ep"), lax.axis_index("tp")
+    row_count, width = mix_in.shape
+    quarter = row_count // parts
+    latent_width = latent_weight.shape[1]
+    half = ROPE // 2
+    first_row = ep * row_count
+
+    def own(array):
+        return lax.dynamic_slice_in_dim(array, tp * quarter, quarter, 0)
+
+    rows = rms_rows(own(ffn_in).astype(f32), ffn_gain).astype(bf16)
+    own_normed = rms_rows(own(mix_in).astype(f32), mix_gain).astype(bf16)
+    latent = rms_rows(jnp.dot(own_normed, latent_weight, preferred_element_type=f32), latent_gain)
+    turned = jnp.dot(own_normed, rotary_weight, preferred_element_type=f32)
+    positions = first_row + jnp.arange(row_count, dtype=jnp.int32)
+    inverse = rope_base ** (-jnp.arange(0, ROPE, 2).astype(f32) / ROPE)
+    angles = positions.astype(f32)[:, None] * inverse[None, :]
+    cosine, sine = jnp.cos(angles), jnp.sin(angles)
+
+    def rotate(vectors, cosine, sine):
+        upper, lower = vectors[..., :half], vectors[..., half:]
+        return jnp.concatenate([upper * cosine - lower * sine, lower * cosine + upper * sine], axis=-1)
+
+    rotary_key = rotate(turned, own(cosine), own(sine))
+    shares = jax.nn.softmax(own(route_scores), axis=-1)
+    named = own(routes)[:, :, None] == jnp.arange(experts, dtype=jnp.int32)[None, None, :]
+    table = jnp.sum(jnp.where(named, shares[:, :, None], 0.0), axis=1)
+    coarse = lax.reduce_precision(table, 8, 7)
+    used = latent_width + ROPE + 2 * experts
+    side_width = -(-used // 128) * 128
+    side = jnp.concatenate(
+        [latent, rotary_key, coarse, table - coarse, jnp.zeros((quarter, side_width - used), f32)],
+        axis=1,
+    ).astype(bf16)
+    normed = rms_rows(mix_in.astype(f32), mix_gain).astype(bf16)
+    head_count = query_weight.shape[1] // (NOPE + ROPE)
+    queries = jnp.dot(normed, query_weight, preferred_element_type=f32).reshape(
+        row_count, head_count, NOPE + ROPE
+    )
+    query_turn = rotate(queries[..., NOPE:], cosine[:, None, :], sine[:, None, :])
+    spare = jnp.zeros((row_count, head_count, side_width - latent_width - ROPE), f32)
+    queries = jnp.concatenate([queries[..., :NOPE], query_turn, spare], axis=-1)
+    queries = queries.astype(bf16).transpose(1, 0, 2)
+    weights = (
+        gate_weight[0], up_weight[0], down_weight[0], key_weight, value_weight, output_weight
+    )
+    mixed, moe_out = layer(rows, side, queries, out_gain, weights, experts, parts)
+    return mixed, moe_out
+
+
 def solution(mesh):
+    experts, parts = mesh.shape["ep"], mesh.shape["tp"]
+
+    def body(*args):
+        quarter, choose = args[10].shape[0] // parts, args[15].shape[1]
+        every_row = 2 * quarter * choose >= quarter * experts
+        paired = parts == 4 and experts % 2 == 0 and (experts // 2) & (experts // 2 - 1) == 0
+        return (dense_local if every_row and paired else local)(*args)
     placed = (
         P("ep", None),
         P(),
@@ -235,7 +617,7 @@
         P("ep", None),
     )
     return jax.shard_map(
-        local,
+        body,
         mesh=mesh,
         in_specs=placed,
         out_specs=(P(("ep", "tp"), None), P(("ep", "tp"), None)),

time: 234 us -> 94.9 us (0.41)
  waiting for transfers between devices: 81.7 us -> 0 us
  Pallas kernels: 0 us -> 69.8 us
  blocking collectives: 60.5 us -> 0 us
  matrix products: 30.5 us -> 6.03 us
  local copies, waits for them, and re-layouts: 26.4 us -> 8.91 us
  between operations: 14 us -> 0.78 us
  starting transfers between devices: 5.68 us -> 0 us
  other arithmetic: 13.9 us -> 8.91 us
    pallas_call x0 -> x1, Pallas kernels: none -> 69.8 us  [layer(): pl.pallas_call(functools.partial(layer_kernel, depth, heads), out_shape=[...]
    reduce_scatter x2 -> x0, waiting for transfers between devices: 45.1 us -> none  [local(): lax.psum_scatter(lax.optimization_barrier(partial_value.astype(jnp.bfloat...]
    all_to_all x1 -> x0, blocking collectives: 32.8 us -> none  [local(): lax.all_to_all(outgoing, 'ep', split_axis=1, concat_axis=1, tiled=True)]
    all_gather x2 -> x0, waiting for transfers between devices: 29.2 us -> none  [the longest x1 29.2 us: local(): row_block = lax.all_gather(arrived, 'tp', axis=0, tiled=True)]
    all_gather x1 -> x0, blocking collectives: 27.7 us -> none  [local(): lax.all_gather(rotary_key, 'ep', axis=1, tiled=True)]
    dot_general x11 -> x3, matrix products: 30.5 us -> 6.03 us  [the longest x1 2.41 us: dense_local(): jnp.dot(normed, query_weight, preferred_element_type=f32)]
    gather x2 -> x0, local copies, waits for them, and re-layouts: 8.07 us -> none  [the longest x1 4.48 us: local(): outgoing = padded[chosen].reshape(capacity, experts, -1)]
    all_to_all x1 -> x0, waiting for transfers between devices: 7.37 us -> none  [local(): lax.all_to_all(result, 'ep', split_axis=1, concat_axis=1, tiled=True)]
  transfers between devices with their start and end apart: 5 -> 0, of which waited for: 4 -> 0; matrix products, arithmetic and copies ran while one was open for 18% -> 0% of each run, Pallas kernels for 0% -> 0%
where the time goes in v2:
time: 94.9 us; the launch traced here: 94.4 us
  Pallas kernels  69.8 us (74%)
  local copies, waits for them, and re-layouts  8.91 us (9%)
  other arithmetic  8.91 us (9%)
  matrix products  6.03 us (6%)
    pallas_call x1, Pallas kernels, layer(): pl.pallas_call(functools.partial(layer_kernel, depth, heads), out_shape=[...  69.8 us
    unnamed x17, local copies, waits for them, and re-layouts  6.54 us
    dot_general x1, matrix products, dense_local(): jnp.dot(normed, query_weight, preferred_element_type=f32)  2.41 us
    reduce_sum x2, other arithmetic, rms_rows(): mean_square = jnp.mean(rows_in * rows_in, axis=-1, keepdims=True)  2.38 us
    dot_general x1, matrix products, dense_local(): jnp.dot(own_normed, latent_weight, preferred_element_type=f32)  2.32 us

profile of v2, /device:TPU:0, one launch (start us, length us, event | category | flops | bytes accessed | tf_op | source)
XLA Modules:
  0.0 94.4 jit_solution(7755099988289293396)
XLA Ops:
  0.6 0.0 copy-start
  0.6 0.0 copy-start.4
  0.7 0.0 copy-start.5
  0.7 0.9 fusion.21
  1.6 0.8 fusion.18
  2.4 0.0 copy-start.3
  2.4 1.2 %fusion = f32[128]{0:T(128)S(1)} fusion(bf16[128,2048]{1,0:T(8,128)(2,1)} %param.17), kind=kLoop, calls=%fused_computation.2 | loop fusion | flops 786304 | bytes 524800 | tf_op jit(solution)/shard_map/reduce_sum | solution.py:21
  3.7 0.1 pad.3.clone
  3.8 0.8 fusion.17
  4.5 1.1 %fusion.7 = (f32[32]{0:T(128)S(1)}, f32[32]{0:T(128)S(1)}) fusion(bf16[128,2048]{1,0:T(8,128)(2,1)} %param.27, s32[]{:T(128)S(6)} %select_n.5, bf16[128,2048]{1,0:T(8,128)(2,1)} %param.17), kind=kLoop, calls=%fused_computation.12 | loop fusion | flops 393152 | bytes 262404 | tf_op jit(solution)/shard_map/reduce_sum | solution.py:21
  5.7 0.8 constant_dynamic-slice_fusion.1
  6.5 0.1 copy.34
  6.5 0.1 copy.33
  6.6 1.3 %fusion.13 = f32[32,64]{1,0:T(8,128)S(1)} fusion(bf16[2048,64]{0,1:T(8,128)(2,1)} %param.21, f32[2048]{0:T(1024)} %param.18, f32[32]{0:T(128)S(1)} %add_rsqrt_fusion.2, bf16[128,2048]{1,0:T(8,128)(2,1)} %param.17, s32[]{:T(128)S(6)} %select_n.5), kind=kOutput, calls=%fused_computation.26 | convolution fusion | flops 8650752 | bytes 409732 | tf_op jit(solution)/shard_map/dot_general | solution.py:555
  7.9 2.3 %multiply_reduce_fusion = (f32[32]{0:T(128)S(1)}, f32[32,512]{1,0:T(8,128)S(1)}) fusion(bf16[2048,512]{1,0:T(8,128)(2,1)} %param.20, f32[2048]{0:T(1024)} %param.18, f32[32]{0:T(128)S(1)} %add_rsqrt_fusion.2, bf16[128,2048]{1,0:T(8,128)(2,1)} %param.17, s32[]{:T(128)S(6)} %select_n.5), kind=kOutput, calls=%fused_computation.25 | convolution fusion | flops 67403744 | bytes 2302212 | tf_op jit(solution)/shard_map/dot_general | solution.py:554
  10.2 0.0 copy-done.5
  10.3 0.1 multiply_convert_fusion
  10.3 0.3 multiply_cosine_fusion
  10.7 0.0 copy-start.1
  10.7 0.0 copy-start.2
  10.7 0.6 copy-done.1
  11.3 0.1 add_convert_fusion.1
  11.4 0.0 copy-done.2
  11.4 0.7 concatenate.8.side_ref
  12.1 0.0 copy-done.4
  12.1 1.7 %fusion.9.row_ref = bf16[32,2048]{1,0:T(8,128)(2,1)} fusion(f32[2048]{0:T(1024)S(1)} %copy-done.4, f32[32]{0:T(128)S(1)} %add_rsqrt_fusion.3, bf16[128,2048]{1,0:T(8,128)(2,1)} %param.27, s32[]{:T(128)S(6)} %select_n.5), kind=kLoop, calls=%fused_computation.14 | loop fusion | flops 262144 | bytes 270468 | tf_op jit(solution)/shard_map/convert_element_type | solution.py:552
  13.7 0.0 copy-done
  13.7 0.0 copy-done.3
  13.7 2.4 %fusion.3 = f32[128,768]{0,1:T(8,128)S(1)} fusion(bf16[2048,768]{1,0:T(8,128)(2,1)S(1)} %copy-done, bf16[128,2048]{1,0:T(8,128)(2,1)} %param.17, f32[2048]{0:T(1024)S(1)} %copy-done.3, f32[128]{0:T(128)S(1)} %add_rsqrt_fusion), kind=kOutput, calls=%fused_computation.5 | convolution fusion | flops 403701760 | bytes 4071936 | tf_op jit(solution)/shard_map/dot_general | solution.py:578
  16.2 0.6 fusion.22
  16.8 0.1 copy.41
  17.0 1.0 %copy.43 = f32[128,4,32]{2,0,1:T(8,128)S(1)} copy(f32[128,4,32]{0,2,1:T(8,128)} %get-tuple-element.4) | data formatting | bytes 131072
  18.0 1.7 %copy.42 = f32[128,4,32]{2,0,1:T(8,128)} copy(f32[128,4,32]{0,2,1:T(8,128)} %get-tuple-element.5) | data formatting | bytes 131072
  19.6 1.1 %subtract_convert_fusion = (bf16[128,4,32]{2,0,1:T(8,128)(2,1)S(1)}, bf16[128,4,32]{2,0,1:T(8,128)(2,1)S(1)}) fusion(f32[128,4,32]{2,0,1:T(8,128)S(1)} %copy.43, f32[128,4,32]{2,0,1:T(8,128)} %copy.42, f32[128,32]{1,0:T(8,128)} %copy-done.2, f32[128,32]{1,0:T(8,128)} %copy-done.1), kind=kLoop, calls=%fused_computation.21 | loop fusion | flops 131072 | bytes 229376 | tf_op jit(solution)/shard_map/convert.1
  20.7 0.8 maximum_bitcast_fusion.query_ref
  21.5 69.8 %layer.1 = (bf16[32,2048]{1,0:T(8,128)(2,1)}, bf16[32,2048]{1,0:T(8,128)(2,1)}) custom-call(bf16[32,2048]{1,0:T(8,128)(2,1)} %fusion.9.row_ref, bf16[32,640]{1,0:T(8,128)(2,1)} %concatenate.8.side_ref, bf16[4,128,256]{2,1,0:T(8,128)(2,1)} %maximum_bitcast_fusion.query_ref, f32[1,2048]{1,0:T(1,128)} %bitcast.15, bf16[2048,256]{1,0:T(8,128)(2,1)} %bitcast.12, ...), custom_call_target="tpu_custom_call" | custom-call | tf_op jit(solution)/shard_map/layer/pallas_call | solution.py:510
  91.3 1.6 %copy.46 = bf16[32,2048]{1,0:T(8,128)(2,1)} copy(bf16[32,2048]{1,0:T(8,128)(2,1)} %get-tuple-element.18) | data formatting | bytes 262144
  92.8 1.6 %copy.47 = bf16[32,2048]{1,0:T(8,128)(2,1)} copy(bf16[32,2048]{1,0:T(8,128)(2,1)} %get-tuple-element.19) | data formatting | bytes 262144
  (12 shorter events, 0.1 us)
Async XLA Ops:
  0.6 13.1 %copy-start = (bf16[2048,768]{1,0:T(8,128)(2,1)S(1)}, bf16[2048,768]{1,0:T(8,128)(2,1)}, u32[]{:S(2)}) copy-start(bf16[2048,768]{1,0:T(8,128)(2,1)} %param.19) | copy-start | bytes 9437188
  0.6 11.4 %copy-start.4 = (f32[2048]{0:T(1024)S(1)}, f32[2048]{0:T(1024)}, u32[]{:S(2)}) copy-start(f32[2048]{0:T(1024)} %param.28) | copy-start | bytes 24580
  0.7 9.6 %copy-start.5 = (f32[512]{0:T(512)S(1)}, f32[512]{0:T(512)}, u32[]{:S(2)}) copy-start(f32[512]{0:T(512)} %param.22) | copy-start | bytes 6148
  2.4 11.3 %copy-start.3 = (f32[2048]{0:T(1024)S(1)}, f32[2048]{0:T(1024)}, u32[]{:S(2)}) copy-start(f32[2048]{0:T(1024)} %param.18) | copy-start | bytes 24580
  10.7 0.6 copy-start.1
  10.7 0.7 copy-start.2
